TPU v7x, 32 devices: a whole 2x2x4 slice. The times are simulated.
32 devices in a mesh: gr: 2 (over x), fs: 8 (over z, y), tp: 2 (over core).
Axes of the slice: x: 2, y: 2, z: 4, core: 2. Of those that a mesh axis runs over, the one named last changes fastest.
Arguments:
- tokens: bfloat16 [2048, 2048], P(('gr', 'tp')), may hold values from -6 to 6
- norm_gain: float32 [2048], P('fs'), may hold values from 0.1 to 1.9
- up_weight: float32 [2048, 8192], P('fs', ('gr', 'tp')), may hold values from -0.125 to 0.125
- down_weight: float32 [8192, 2048], P('fs', ('gr', 'tp')), may hold values from -0.09375 to 0.09375
Outputs:
- sampler_up: bfloat16 [2048, 8192], P(None, 'fs')
- sampler_down: bfloat16 [8192, 2048], P('fs')
- mixed: bfloat16 [2048, 2048], P(('gr', 'tp'), 'fs')
All inputs are finite; a program needn't handle non-finite values.
Results may differ from a plain program's by a relative error of at most 0.023.
Values may be sent and summed in bfloat16 or wider, within the bound.
A program may use at most 64 MiB of HBM per device.

v0:
```python
import jax
import jax.numpy as jnp
from jax import lax
from jax.sharding import PartitionSpec as P


def per_device(tokens, norm_gain, up_weight, down_weight):
    up_scaled = (norm_gain[:, None] * up_weight).astype(jnp.bfloat16)
    down_half = down_weight.astype(jnp.bfloat16)
    up_columns, down_columns = (
        lax.all_gather(up_scaled, ("gr", "tp"), axis=1, tiled=True),
        lax.all_gather(down_half, ("gr", "tp"), axis=1, tiled=True),
    )
    up_block = lax.all_to_all(up_columns, "fs", split_axis=1, concat_axis=0, tiled=True)
    widened = tokens.astype(jnp.float32)
    normed = (
        widened * lax.rsqrt(jnp.mean(widened * widened, axis=-1, keepdims=True) + 1e-06)
    ).astype(jnp.bfloat16)
    preact = jnp.dot(normed, up_block, preferred_element_type=jnp.float32)
    hidden = jnp.square(jax.nn.relu(preact)).astype(jnp.bfloat16)
    summed = lax.psum_scatter(
        lax.dot_general(
            down_columns, hidden, (((0,), (1,)), ((), ())), preferred_element_type=jnp.float32
        ).astype(jnp.bfloat16),
        "fs",
        scatter_dimension=0,
        tiled=True,
    )
    mixed = summed.T
    return (up_block, down_columns, mixed)


def solution(mesh):
    in_specs = (P(("gr", "tp"), None), P("fs"), P("fs", ("gr", "tp")), P("fs", ("gr", "tp")))
    out_specs = (P(None, "fs"), P("fs", None), P(("gr", "tp"), "fs"))
    return jax.shard_map(
        per_device, mesh=mesh, in_specs=in_specs, out_specs=out_specs, check_vma=False
    )
```

profile of v0, /device:TPU:0, one launch (start us, length us, event | category | flops | bytes accessed | tf_op | source)
XLA Modules:
  0.0 242.2 jit_solution(8741351901346556773)
XLA Ops:
  7.2 0.0 all-gather.3.cloned.1.call-start
  7.2 2.7 %multiply_convert_fusion.1 = bf16[256,2048]{1,0:T(8,128)(2,1)} fusion(f32[256,2048]{1,0:T(8,128)} %param.6, f32[256]{0:T(256)} %param.5), kind=kLoop, calls=%fused_computation.10 | loop fusion | flops 1048576 | bytes 3146752 | tf_op jit(solution)/shard_map/convert_element_type | solution.py:8
  10.0 0.0 all-gather.3.cloned.1.call-update
  10.0 37.3 %all-gather.3.cloned.1.call-done = bf16[256,8192]{1,0:T(8,128)(2,1)} async-done(((bf16[256,2048]{1,0:T(8,128)(2,1)}), bf16[256,8192]{1,0:T(8,128)(2,1)}) %all-gather.3.cloned.1.call-update) | async-done | bytes 4194320 | tf_op jit(solution)/shard_map/all_gather | solution.py:11
  47.3 4.8 %copy.10 = bf16[32,8,8,1024]{3,2,0,1:T(8,128)(2,1)} copy(bf16[32,8,8,1024]{3,2,1,0:T(8,128)(2,1)} %bitcast.13) | data formatting | bytes 8388608 | tf_op jit(solution)/shard_map/all_to_all | solution.py:14
  52.1 0.0 copy-start.1
  52.1 5.6 %all-to-all-start = ((bf16[256,8,1024]{2,0,1:T(8,128)(2,1)}), bf16[256,8,1024]{2,0,1:T(8,128)(2,1)}, u32[]{:S(2)}, u32[]{:S(2)}) async-start(bf16[256,8,1024]{2,0,1:T(8,128)(2,1)} %bitcast.12), calls=%async_computation | async-start | bytes 8388608 | tf_op jit(solution)/shard_map/all_to_all | solution.py:14
  57.8 0.0 all-gather.5.cloned.1.call-start
  57.8 0.0 copy-done.1
  57.9 1.1 convert_element_type.22
  59.0 0.0 all-gather.5.cloned.1.call-update
  59.0 0.0 reduce-scatter.2.cloned.1.call-start
  59.0 2.1 fusion
  61.1 34.6 %all-gather.5.cloned.1.call-done = bf16[1024,2048]{1,0:T(8,128)(2,1)} async-done(((bf16[1024,512]{1,0:T(8,128)(2,1)}), bf16[1024,2048]{1,0:T(8,128)(2,1)}) %all-gather.5.cloned.1.call-update) | async-done | bytes 4194320 | tf_op jit(solution)/shard_map/all_gather | solution.py:12
  95.7 55.8 %all-to-all-done = bf16[256,8,1024]{2,0,1:T(8,128)(2,1)} async-done(((bf16[256,8,1024]{2,0,1:T(8,128)(2,1)}), bf16[256,8,1024]{2,0,1:T(8,128)(2,1)}, u32[]{:S(2)}, u32[]{:S(2)}) %all-to-all-start) | async-done | bytes 4194336 | tf_op jit(solution)/shard_map/all_to_all | solution.py:14
  151.5 9.9 %fusion.2 = bf16[2048,512]{0,1:T(8,128)(2,1)} fusion(bf16[1024,2048]{1,0:T(8,128)(2,1)} %all-gather.5.cloned.1.call-done, bf16[2048,1024]{1,0:T(8,128)(2,1)} %bitcast.1, bf16[512,2048]{1,0:T(8,128)(2,1)} %param.4, f32[512]{0:T(512)S(1)} %add_rsqrt_fusion), kind=kOutput, calls=%fused_computation.6 | convolution fusion | flops 4300734464 | bytes 12584960 | tf_op jit(solution)/shard_map/dot_general | solution.py:22
  161.4 0.0 reduce-scatter.2.cloned.1.call-update
  161.4 67.4 %reduce-scatter.2.cloned.1.call-done = bf16[256,512]{0,1:T(8,128)(2,1)} async-done(((bf16[2048,512]{0,1:T(8,128)(2,1)}), bf16[256,512]{0,1:T(8,128)(2,1)}) %reduce-scatter.2.cloned.1.call-update) | async-done | bytes 262160 | tf_op jit(solution)/shard_map/reduce_scatter | solution.py:21
  228.8 0.0 copy-start
  228.8 4.8 %copy.13 = bf16[2048,1024]{1,0:T(8,128)(2,1)} copy(bf16[2048,1024]{1,0:T(8,128)(2,1)} %bitcast.1) | data formatting | bytes 8388608
  233.7 0.0 copy-done
  233.7 2.0 copy.14
  (1 shorter events, 0.0 us)
Async XLA Ops:
  7.2 40.2 %all-gather.3.cloned.1.call-start = ((), (), s32[]{:S(2)}) async-start(), calls=%async_computation.2 | async-start | bytes 5242880 | tf_op jit(solution)/shard_map/all_gather | solution.py:11
  52.1 5.7 %copy-start.1 = (f32[1024,512]{1,0:T(8,128)S(1)}, f32[1024,512]{1,0:T(8,128)}, u32[]{:S(2)}) copy-start(f32[1024,512]{1,0:T(8,128)} %param.7) | copy-start | bytes 6291460
  52.1 99.3 %all-to-all-start = ((bf16[256,8,1024]{2,0,1:T(8,128)(2,1)}), bf16[256,8,1024]{2,0,1:T(8,128)(2,1)}, u32[]{:S(2)}, u32[]{:S(2)}) async-start(bf16[256,8,1024]{2,0,1:T(8,128)(2,1)} %bitcast.12), calls=%async_computation | async-start | bytes 8388608 | tf_op jit(solution)/shard_map/all_to_all | solution.py:14
  57.8 37.9 %all-gather.5.cloned.1.call-start = ((), (), s32[]{:S(2)}) async-start(), calls=%async_computation.3 | async-start | bytes 5242880 | tf_op jit(solution)/shard_map/all_gather | solution.py:12
  59.0 169.9 %reduce-scatter.2.cloned.1.call-start = ((), (), s32[]{:S(2)}) async-start(), calls=%async_computation.4 | async-start | bytes 2359296 | tf_op jit(solution)/shard_map/reduce_scatter | solution.py:21
  228.8 4.8 %copy-start = (bf16[1024,2048]{1,0:T(8,128)(2,1)S(1)}, bf16[1024,2048]{1,0:T(8,128)(2,1)}, u32[]{:S(2)}) copy-start(bf16[1024,2048]{1,0:T(8,128)(2,1)} %all-gather.5.cloned.1.call-done) | copy-start | bytes 12582916
Sparse Core Ops, SparseCore 0:
  10.1 37.1 all-gather.2
  60.7 34.9 all-gather.4
  161.6 67.2 reduce-scatter.1
where the time goes:
time: 243 us; the launch traced here: 242 us
  waiting for transfers between devices  195 us (80%)
  between operations  13.8 us (6%)
  local copies, waits for them, and re-layouts  11.7 us (5%)
  matrix products  9.92 us (4%)
  other arithmetic  5.93 us (2%)
  starting transfers between devices  5.77 us (2%)
    reduce_scatter x1, waiting for transfers between devices, per_device(): lax.psum_scatter(lax.dot_general(down_columns, hidden, (((0,), (1,)), (()...  67.4 us
    all_to_all x1, waiting for transfers between devices, per_device(): lax.all_to_all(up_columns, 'fs', split_axis=1, concat_axis=0, tiled=True)  55.8 us
    all_gather x1, waiting for transfers between devices, per_device(): lax.all_gather(up_scaled, ('gr', 'tp'), axis=1, tiled=True)  37.3 us
    all_gather x1, waiting for transfers between devices, per_device(): lax.all_gather(down_half, ('gr', 'tp'), axis=1, tiled=True)  34.6 us
    dot_general x1, matrix products, per_device(): lax.dot_general(down_columns, hidden, (((0,), (1,)), ((), ())), preferred...  9.92 us
    unnamed x6, local copies, waits for them, and re-layouts  6.83 us
    all_to_all x1, starting transfers between devices, per_device(): lax.all_to_all(up_columns, 'fs', split_axis=1, concat_axis=0, tiled=True)  5.65 us
  transfers between devices with their start and end apart: 4, of which 4 were waited for; matrix products, arithmetic and copies ran while one was open for 1% of the time, Pallas kernels for 0%

commit v1 on v0

v1 whole, which is shorter than its diff:
```python
import functools

import jax
import jax.numpy as jnp
from jax import lax
from jax.experimental import pallas as pl
from jax.experimental.pallas import tpu as pltpu
from jax.sharding import PartitionSpec as P

MESH = pl.DeviceIdType.MESH
VMEM_LIMIT = 60 * 1024 * 1024


def flipped(index, step, count):
    if count & (count - 1):
        return lax.rem(index + step, count)
    bit = 1
    while bit < count:
        if step & bit:
            index = index + (1 - 2 * lax.rem(index // bit, 2)) * bit
        bit *= 2
    return index


def remote(src, dst, send, recv, device):
    return pltpu.make_async_remote_copy(
        src_ref=src, dst_ref=dst, send_sem=send, recv_sem=recv,
        device_id=device, device_id_type=MESH,
    )


def gather_kernel(
    tp, blocks, shards, tokens, gain, up, down, up_out, down_out, hidden_out,
    gath, normed, acc, xs, xr, fsend, frecv, ps, pr, ds_, dr, pds, pdr,
):
    g, f, t = lax.axis_index("gr"), lax.axis_index("fs"), lax.axis_index("tp")
    per = tp // 2
    chips = gath.shape[0]
    c, k = g * per + t // 2, lax.rem(t, 2)
    rows, width = up.shape
    half = rows // 2
    block = width // blocks
    cols = down.shape[1]

    def dev(chip, shard, core):
        return (chip // per, shard, lax.rem(chip, per) * 2 + core)

    def down_cols(chip, core):
        return pl.ds(pl.multiple_of((chip * 2 + core) * cols, cols), cols)

    barrier = pltpu.get_barrier_semaphore()
    for s in range(1, chips):
        pl.semaphore_signal(
            barrier, inc=1, device_id=dev(lax.rem(c + s, chips), f, k), device_id_type=MESH
        )
    for s in range(shards):
        for core in range(2):
            if s == 0 and core == 0:
                continue
            other = lax.rem(f + s, shards)
            core_id = lax.rem(k + core, 2)
            pl.semaphore_signal(
                barrier, inc=1, device_id=dev(c, other, core_id), device_id_type=MESH
            )

    gath[c] = (gain[...] * up[...]).astype(jnp.bfloat16)
    down_out[:, down_cols(c, k)] = down[...].astype(jnp.bfloat16)
    pl.semaphore_wait(barrier, chips - 1 + 2 * shards - 1)

    def unit(chip, j, h):
        return gath.at[chip, pl.ds(h * half, half), pl.ds(j * block, block)]

    def up_rows(shard, core):
        return up_out.at[pl.ds(pl.multiple_of(shard * rows + core * half, half), half), :]

    def target(chip, j):
        return (chip * 2 + k) * blocks + j

    def forward(chip, j, h):
        to = target(chip, j)
        return remote(
            unit(chip, j, h), up_rows(f, h), fsend.at[chip, j, h], frecv.at[f], dev(c, to, h)
        )

    def stays(chip, j, h):
        return jnp.logical_and(target(chip, j) == f, k == h)

    def start_forward(chip, j, h):
        @pl.when(jnp.logical_not(stays(chip, j, h)))
        def _():
            forward(chip, j, h).start()

        @pl.when(stays(chip, j, h))
        def _():
            up_rows(f, h)[...] = unit(chip, j, h)[...]

    def exchange(s, j, h):
        return remote(
            unit(c, j, h), unit(c, j, h), xs.at[s, j, h], xr.at[s, j, h],
            dev(lax.rem(c + s, chips), f, k),
        )

    def exchanged(s, j, h):
        source = lax.rem(c + chips - s, chips)
        return remote(
            unit(source, j, h), unit(source, j, h), xs.at[s, j, h], xr.at[s, j, h], dev(c, f, k)
        )

    def down_copy(s):
        mine = down_out.at[:, down_cols(c, k)]
        return remote(mine, mine, ds_.at[s], dr.at[s], dev(lax.rem(c + s, chips), f, k))

    def down_relay(s, core):
        held = down_out.at[:, down_cols(lax.rem(c + chips - s, chips), core)]
        return remote(held, held, pds.at[s], pdr.at[s], dev(c, f, 1 - k))

    units = [(j, h) for h in range(2) for j in range(blocks)]
    for j, h in units:
        for s in range(1, chips):
            exchange(s, j, h).start()
        start_forward(c, j, h)
    for s in range(1, chips):
        down_copy(s).start()
    down_relay(0, k).start()

    widened = tokens[...].astype(jnp.float32)
    scale = lax.rsqrt(jnp.mean(widened * widened, axis=-1, keepdims=True) + 1e-06)
    for shard in range(shards):
        part = tokens[:, shard * rows:(shard + 1) * rows].astype(jnp.float32)
        normed[shard] = (part * scale).astype(jnp.bfloat16)

    for j, h in units:
        for s in range(1, chips):
            exchanged(s, j, h).wait_recv()
            start_forward(lax.rem(c + chips - s, chips), j, h)

    source_core = lax.rem(f // blocks, 2)
    own_stays = source_core == k

    def arrival(shard):
        return remote(
            up_rows(shard, k), up_rows(shard, k), ps.at[shard], frecv.at[shard], dev(c, f, 1 - k)
        )

    def relay(shard, core):
        held = up_rows(shard, core)
        return remote(held, held, ps.at[shard], pr.at[shard], dev(c, f, 1 - k))

    def accumulate(shard, first):
        weights = up_out[pl.ds(pl.multiple_of(shard * rows, rows), rows), :]
        product = jnp.dot(normed[shard], weights, preferred_element_type=jnp.float32)
        if first:
            acc[...] = product
        else:
            acc[...] += product

    order = [flipped(f, s, shards) for s in list(range(1, shards)) + [0]]
    for position, shard in enumerate(order):
        if position < shards - 1:
            arrival(shard).wait_recv()
        else:
            @pl.when(jnp.logical_not(own_stays))
            def _():
                arrival(shard).wait_recv()
        relay(shard, k).start()
        if position > 0:
            before = order[position - 1]
            relay(before, 1 - k).wait_recv()
            accumulate(before, position == 1)
    for s in range(1, chips):
        down_copy_in = remote(
            down_out.at[:, down_cols(lax.rem(c + chips - s, chips), k)],
            down_out.at[:, down_cols(lax.rem(c + chips - s, chips), k)],
            ds_.at[s], dr.at[s], dev(c, f, 1 - k),
        )
        down_copy_in.wait_recv()
        down_relay(s, k).start()
    relay(order[-1], 1 - k).wait_recv()
    accumulate(order[-1], False)
    hidden_out[...] = jnp.square(jnp.maximum(acc[...], 0.0)).astype(jnp.bfloat16)

    for s in range(chips):
        down_relay(s, 1 - k).wait_recv()
        down_relay(s, k).wait_send()
    for s in range(1, chips):
        down_copy(s).wait_send()
        for j, h in units:
            exchange(s, j, h).wait_send()
    for shard in order:
        relay(shard, k).wait_send()
    for s in range(chips):
        chip = lax.rem(c + s, chips)
        for j, h in units:
            @pl.when(jnp.logical_not(stays(chip, j, h)))
            def _():
                forward(chip, j, h).wait_send()


def reduce_kernel(hidden, down, mixed, part, ybuf, zout, zbuf, ys, yr, zs, zr):
    g, f, t = lax.axis_index("gr"), lax.axis_index("fs"), lax.axis_index("tp")
    pairs = ybuf.shape[0]
    wide = mixed.shape[1]
    z, y = f // 2, lax.rem(f, 2)

    barrier = pltpu.get_barrier_semaphore()
    pl.semaphore_signal(
        barrier, inc=1, device_id=(g, z * 2 + 1 - y, t), device_id_type=MESH
    )
    for s in range(1, pairs):
        pl.semaphore_signal(
            barrier, inc=1, device_id=(g, lax.rem(z + s, pairs) * 2 + y, t), device_id_type=MESH
        )
    order = [flipped(z, s, pairs) for s in list(range(pairs - 1, 0, -1)) + [0]]

    def compute(pair):
        columns = pl.ds(pl.multiple_of(pair * 2 * wide, 2 * wide), 2 * wide)
        both = jnp.dot(hidden[...], down[:, columns], preferred_element_type=jnp.float32)
        both = both.astype(jnp.bfloat16)
        part[2 * pair] = both[:, :wide]
        part[2 * pair + 1] = both[:, wide:]

    def across(pair):
        return remote(
            part.at[2 * pair + 1 - y], ybuf.at[pair], ys.at[pair], yr.at[pair],
            (g, z * 2 + 1 - y, t),
        )

    def along(pair, sender):
        return remote(
            zout.at[pair], zbuf.at[sender], zs.at[pair], zr.at[sender], (g, pair * 2 + y, t)
        )

    compute(order[0])
    pl.semaphore_wait(barrier, pairs)
    for position in range(1, pairs):
        compute(order[position])
        across(order[position - 1]).start()
    across(order[-1]).start()

    previous = None
    for pair in order[:-1]:
        across(pair).wait_recv()
        zout[pair] = (
            part[2 * pair + y].astype(jnp.float32) + ybuf[pair].astype(jnp.float32)
        ).astype(jnp.bfloat16)
        along(pair, z).start()
    across(order[-1]).wait_recv()
    total = part[2 * z + y].astype(jnp.float32) + ybuf[z].astype(jnp.float32)
    for pair in order[-2::-1]:
        along(z, pair).wait_recv()
        total = total + zbuf[pair].astype(jnp.float32)
    mixed[...] = total.astype(jnp.bfloat16)
    for pair in order:
        across(pair).wait_send()
    for pair in order[:-1]:
        along(pair, z).wait_send()


def per_device(gr, fs, tp, tokens, norm_gain, up_weight, down_weight):
    rows, width = up_weight.shape
    units, cols = down_weight.shape
    group = gr * tp
    chips = group // 2
    block = width * group // fs
    blocks = width // block
    count, depth = tokens.shape
    model = cols * group
    vmem = pl.BlockSpec(memory_space=pltpu.VMEM)
    bf16, f32 = jnp.bfloat16, jnp.float32
    dma = pltpu.SemaphoreType.DMA
    up_block, down_columns, hidden = pl.pallas_call(
        functools.partial(gather_kernel, tp, blocks, fs),
        out_shape=(
            jax.ShapeDtypeStruct((depth, block), bf16),
            jax.ShapeDtypeStruct((units, model), bf16),
            jax.ShapeDtypeStruct((count, block), bf16),
        ),
        in_specs=[vmem] * 4,
        out_specs=(vmem,) * 3,
        scratch_shapes=[
            pltpu.VMEM((chips, rows, width), bf16),
            pltpu.VMEM((fs, count, rows), bf16),
            pltpu.VMEM((count, block), f32),
            dma((chips, blocks, 2)), dma((chips, blocks, 2)),
            dma((chips, blocks, 2)), dma((fs,)),
            dma((fs,)), dma((fs,)),
            dma((chips,)), dma((chips,)), dma((chips,)), dma((chips,)),
        ],
        compiler_params=pltpu.CompilerParams(
            collective_id=0, has_side_effects=True, vmem_limit_bytes=VMEM_LIMIT
        ),
    )(tokens, norm_gain[:, None], up_weight, down_weight)
    pairs = fs // 2
    wide = model // fs
    mixed = pl.pallas_call(
        reduce_kernel,
        out_shape=jax.ShapeDtypeStruct((count, wide), bf16),
        in_specs=[vmem] * 2,
        out_specs=vmem,
        scratch_shapes=[
            pltpu.VMEM((fs, count, wide), bf16),
            pltpu.VMEM((pairs, count, wide), bf16),
            pltpu.VMEM((pairs, count, wide), bf16),
            pltpu.VMEM((pairs, count, wide), bf16),
            dma((pairs,)), dma((pairs,)), dma((pairs,)), dma((pairs,)),
        ],
        compiler_params=pltpu.CompilerParams(
            collective_id=1, has_side_effects=True, vmem_limit_bytes=VMEM_LIMIT
        ),
    )(hidden, down_columns)
    return (up_block, down_columns, mixed)


def solution(mesh):
    in_specs = (P(("gr", "tp"), None), P("fs"), P("fs", ("gr", "tp")), P("fs", ("gr", "tp")))
    out_specs = (P(None, "fs"), P("fs", None), P(("gr", "tp"), "fs"))
    body = functools.partial(per_device, mesh.shape["gr"], mesh.shape["fs"], mesh.shape["tp"])
    return jax.shard_map(
        body, mesh=mesh, in_specs=in_specs, out_specs=out_specs, check_vma=False
    )
```

time: 243 us -> 118 us (0.49)
  waiting for transfers between devices: 195 us -> 0 us
  Pallas kernels: 0 us -> 108 us
  between operations: 13.8 us -> 0.66 us
  matrix products: 9.92 us -> 0 us
  other arithmetic: 5.93 us -> 0 us
  starting transfers between devices: 5.77 us -> 0 us
  local copies, waits for them, and re-layouts: 11.7 us -> 9.01 us
    pallas_call x0 -> x2, Pallas kernels: none -> 108 us  [the longest x1 62.8 us: per_device(): pl.pallas_call(functools.partial(gather_kernel, tp, blocks, fs), out_shap...]
    all_gather x2 -> x0, waiting for transfers between devices: 71.9 us -> none  [the longest x1 37.3 us: per_device(): lax.all_gather(up_scaled, ('gr', 'tp'), axis=1, tiled=True)]
    reduce_scatter x1 -> x0, waiting for transfers between devices: 67.4 us -> none  [per_device(): lax.psum_scatter(lax.dot_general(down_columns, hidden, (((0,), (1,)), (()...]
    all_to_all x1 -> x0, waiting for transfers between devices: 55.8 us -> none  [per_device(): lax.all_to_all(up_columns, 'fs', split_axis=1, concat_axis=0, tiled=True)]
    dot_general x1 -> x0, matrix products: 9.92 us -> none  [per_device(): lax.dot_general(down_columns, hidden, (((0,), (1,)), ((), ())), preferred...]
    all_to_all x1 -> x0, starting transfers between devices: 5.65 us -> none  [per_device(): lax.all_to_all(up_columns, 'fs', split_axis=1, concat_axis=0, tiled=True)]
    all_to_all x1 -> x0, local copies, waits for them, and re-layouts: 4.83 us -> none  [per_device(): lax.all_to_all(up_columns, 'fs', split_axis=1, concat_axis=0, tiled=True)]
    convert_element_type x2 -> x0, other arithmetic: 3.85 us -> none  [the longest x1 2.74 us: per_device(): up_scaled = (norm_gain[:, None] * up_weight).astype(jnp.bfloat16)]
  transfers between devices with their start and end apart: 4 -> 0, of which waited for: 4 -> 0; matrix products, arithmetic and copies ran while one was open for 1% -> 0% of each run, Pallas kernels for 0% -> 0%
where the time goes in v1:
time: 118 us
  Pallas kernels  108 us (92%)
  local copies, waits for them, and re-layouts  9.01 us (8%)
    pallas_call x1, Pallas kernels, per_device(): pl.pallas_call(functools.partial(gather_kernel, tp, blocks, fs), out_shap...  62.8 us
    pallas_call x1, Pallas kernels, per_device(): pl.pallas_call(reduce_kernel, out_shape=jax.ShapeDtypeStruct((count, wide...  45.5 us
    unnamed x7, local copies, waits for them, and re-layouts  7.54 us

profile of v1, /device:TPU:0, one launch (start us, length us, event | category | flops | bytes accessed | tf_op | source)
XLA Modules:
  0.0 118.0 jit_solution(7943823810944911766)
XLA Ops:
  0.6 1.5 %copy.7.gain = f32[256,1]{1,0:T(8,128)} copy(f32[256,1]{0,1:T(1,128)} %bitcast.1) | data formatting | bytes 2048 | tf_op jit(solution)/shard_map/broadcast_in_dim | solution.py:292
  2.1 62.8 %shard_map.67 = (bf16[2048,1024]{1,0:T(8,128)(2,1)}, bf16[1024,2048]{1,0:T(8,128)(2,1)}, bf16[512,1024]{1,0:T(8,128)(2,1)}) custom-call(bf16[512,2048]{1,0:T(8,128)(2,1)} %tokens.1, f32[256,1]{1,0:T(8,128)} %copy.7.gain, f32[256,2048]{1,0:T(8,128)} %up.1, f32[1024,512]{1,0:T(8,128)} %down.1), custom_call_target="tpu_custom_call" | custom-call | tf_op jit(solution)/shard_map/pallas_call | solution.py:271
  64.9 45.5 %shard_map.68 = bf16[512,256]{1,0:T(8,128)(2,1)} custom-call(bf16[512,1024]{1,0:T(8,128)(2,1)} %get-tuple-element.8.hidden, bf16[1024,2048]{1,0:T(8,128)(2,1)} %get-tuple-element.13.down), custom_call_target="tpu_custom_call" | custom-call | tf_op jit(solution)/shard_map/pallas_call | solution.py:295
  110.5 0.0 copy-start
  110.5 4.8 %copy.11 = bf16[2048,1024]{1,0:T(8,128)(2,1)} copy(bf16[2048,1024]{1,0:T(8,128)(2,1)} %get-tuple-element.12) | data formatting | bytes 8388608
  115.3 0.0 copy-done
  115.3 0.0 copy-start.1
  115.3 2.0 %copy.12 = bf16[1024,2048]{1,0:T(8,128)(2,1)} copy(bf16[1024,2048]{1,0:T(8,128)(2,1)S(1)} %copy-done) | data formatting | bytes 8388608
  117.3 0.0 copy-done.1
  117.3 0.7 copy.13
Async XLA Ops:
  110.5 4.8 %copy-start = (bf16[1024,2048]{1,0:T(8,128)(2,1)S(1)}, bf16[1024,2048]{1,0:T(8,128)(2,1)}, u32[]{:S(2)}) copy-start(bf16[1024,2048]{1,0:T(8,128)(2,1)} %get-tuple-element.13.down) | copy-start | bytes 12582916
  115.3 2.0 %copy-start.1 = (bf16[512,256]{1,0:T(8,128)(2,1)S(1)}, bf16[512,256]{1,0:T(8,128)(2,1)}, u32[]{:S(2)}) copy-start(bf16[512,256]{1,0:T(8,128)(2,1)} %shard_map.68) | copy-start | bytes 786436

commit v2 on v1

--- a/solution.py
+++ b/solution.py
@@ -8,7 +8,11 @@
 from jax.sharding import PartitionSpec as P
 
 MESH = pl.DeviceIdType.MESH
-VMEM_LIMIT = 60 * 1024 * 1024
+MIB = 1024 * 1024
+GATHER_VMEM = 32
+REDUCE_VMEM = 20
+SLICES = 2
+PIECES = 2
 
 
 def flipped(index, step, count):
@@ -63,12 +67,18 @@
                 barrier, inc=1, device_id=dev(c, other, core_id), device_id_type=MESH
             )
 
-    gath[c] = (gain[...] * up[...]).astype(jnp.bfloat16)
+    square = (rows, rows)
+    diagonal = lax.broadcasted_iota(jnp.int32, square, 0) == lax.broadcasted_iota(jnp.int32, square, 1)
+    column = jnp.sum(jnp.where(diagonal, gain[...], 0.0), axis=1, keepdims=True)
+    gath[c] = (column * up[...]).astype(jnp.bfloat16)
     down_out[:, down_cols(c, k)] = down[...].astype(jnp.bfloat16)
     pl.semaphore_wait(barrier, chips - 1 + 2 * shards - 1)
 
-    def unit(chip, j, h):
-        return gath.at[chip, pl.ds(h * half, half), pl.ds(j * block, block)]
+    slices = xs.shape[2] // 2
+    piece = half // slices
+
+    def unit(chip, j, u):
+        return gath.at[chip, pl.ds(u * piece, piece), pl.ds(j * block, block)]
 
     def up_rows(shard, core):
         return up_out.at[pl.ds(pl.multiple_of(shard * rows + core * half, half), half), :]
@@ -76,14 +86,18 @@
     def target(chip, j):
         return (chip * 2 + k) * blocks + j
 
-    def forward(chip, j, h):
+    def landing(u):
+        return up_out.at[pl.ds(pl.multiple_of(f * rows + u * piece, piece), piece), :]
+
+    def forward(chip, j, u):
         to = target(chip, j)
         return remote(
-            unit(chip, j, h), up_rows(f, h), fsend.at[chip, j, h], frecv.at[f], dev(c, to, h)
-        )
-
-    def stays(chip, j, h):
-        return jnp.logical_and(target(chip, j) == f, k == h)
+            unit(chip, j, u), landing(u), fsend.at[chip, j, u], frecv.at[f],
+            dev(c, to, u // slices),
+        )
+
+    def stays(chip, j, u):
+        return jnp.logical_and(target(chip, j) == f, k == u // slices)
 
     def start_forward(chip, j, h):
         @pl.when(jnp.logical_not(stays(chip, j, h)))
@@ -92,7 +106,7 @@
 
         @pl.when(stays(chip, j, h))
         def _():
-            up_rows(f, h)[...] = unit(chip, j, h)[...]
+            landing(h)[...] = unit(chip, j, h)[...]
 
     def exchange(s, j, h):
         return remote(
@@ -114,7 +128,7 @@
         held = down_out.at[:, down_cols(lax.rem(c + chips - s, chips), core)]
         return remote(held, held, pds.at[s], pdr.at[s], dev(c, f, 1 - k))
 
-    units = [(j, h) for h in range(2) for j in range(blocks)]
+    units = [(j, q + core * slices) for q in range(slices) for core in range(2) for j in range(blocks)]
     for j, h in units:
         for s in range(1, chips):
             exchange(s, j, h).start()
@@ -219,41 +233,53 @@
         part[2 * pair] = both[:, :wide]
         part[2 * pair + 1] = both[:, wide:]
 
-    def across(pair):
-        return remote(
-            part.at[2 * pair + 1 - y], ybuf.at[pair], ys.at[pair], yr.at[pair],
-            (g, z * 2 + 1 - y, t),
-        )
-
-    def along(pair, sender):
-        return remote(
-            zout.at[pair], zbuf.at[sender], zs.at[pair], zr.at[sender], (g, pair * 2 + y, t)
+    pieces = ys.shape[1]
+    span = mixed.shape[0] // pieces
+
+    def across(pair, i):
+        tokens = pl.ds(i * span, span)
+        return remote(
+            part.at[2 * pair + 1 - y, tokens], ybuf.at[pair, tokens], ys.at[pair, i],
+            yr.at[pair, i], (g, z * 2 + 1 - y, t),
+        )
+
+    def along(pair, sender, i):
+        tokens = pl.ds(i * span, span)
+        return remote(
+            zout.at[pair, tokens], zbuf.at[sender, tokens], zs.at[pair, i], zr.at[sender, i],
+            (g, pair * 2 + y, t),
         )
 
     compute(order[0])
     pl.semaphore_wait(barrier, pairs)
-    for position in range(1, pairs):
-        compute(order[position])
-        across(order[position - 1]).start()
-    across(order[-1]).start()
-
-    previous = None
+    for position in range(1, pairs + 1):
+        if position < pairs:
+            compute(order[position])
+        for i in range(pieces):
+            across(order[position - 1], i).start()
+
+    def summed(pair, i):
+        tokens = pl.ds(i * span, span)
+        return part[2 * pair + y, tokens].astype(jnp.float32) + ybuf[pair, tokens].astype(jnp.float32)
+
     for pair in order[:-1]:
-        across(pair).wait_recv()
-        zout[pair] = (
-            part[2 * pair + y].astype(jnp.float32) + ybuf[pair].astype(jnp.float32)
-        ).astype(jnp.bfloat16)
-        along(pair, z).start()
-    across(order[-1]).wait_recv()
-    total = part[2 * z + y].astype(jnp.float32) + ybuf[z].astype(jnp.float32)
-    for pair in order[-2::-1]:
-        along(z, pair).wait_recv()
-        total = total + zbuf[pair].astype(jnp.float32)
-    mixed[...] = total.astype(jnp.bfloat16)
-    for pair in order:
-        across(pair).wait_send()
-    for pair in order[:-1]:
-        along(pair, z).wait_send()
+        for i in range(pieces):
+            across(pair, i).wait_recv()
+            zout[pair, pl.ds(i * span, span)] = summed(pair, i).astype(jnp.bfloat16)
+            along(pair, z, i).start()
+    for i in range(pieces):
+        tokens = pl.ds(i * span, span)
+        across(z, i).wait_recv()
+        total = summed(z, i)
+        for pair in order[:-1]:
+            along(z, pair, i).wait_recv()
+            total = total + zbuf[pair, tokens].astype(jnp.float32)
+        mixed[tokens] = total.astype(jnp.bfloat16)
+    for i in range(pieces):
+        for pair in order:
+            across(pair, i).wait_send()
+        for pair in order[:-1]:
+            along(pair, z, i).wait_send()
 
 
 def per_device(gr, fs, tp, tokens, norm_gain, up_weight, down_weight):
@@ -281,15 +307,17 @@
             pltpu.VMEM((chips, rows, width), bf16),
             pltpu.VMEM((fs, count, rows), bf16),
             pltpu.VMEM((count, block), f32),
-            dma((chips, blocks, 2)), dma((chips, blocks, 2)),
-            dma((chips, blocks, 2)), dma((fs,)),
+            *[dma((chips, blocks, 2 * SLICES)) for _ in range(3)], dma((fs,)),
             dma((fs,)), dma((fs,)),
             dma((chips,)), dma((chips,)), dma((chips,)), dma((chips,)),
         ],
         compiler_params=pltpu.CompilerParams(
-            collective_id=0, has_side_effects=True, vmem_limit_bytes=VMEM_LIMIT
-        ),
-    )(tokens, norm_gain[:, None], up_weight, down_weight)
+            collective_id=0, has_side_effects=True, vmem_limit_bytes=GATHER_VMEM * MIB
+        ),
+        cost_estimate=pl.CostEstimate(
+            flops=2 * count * depth * block, bytes_accessed=160 * MIB, transcendentals=0
+        ),
+    )(tokens, norm_gain[None, :], up_weight, down_weight)
     pairs = fs // 2
     wide = model // fs
     mixed = pl.pallas_call(
@@ -302,10 +330,13 @@
             pltpu.VMEM((pairs, count, wide), bf16),
             pltpu.VMEM((pairs, count, wide), bf16),
             pltpu.VMEM((pairs, count, wide), bf16),
-            dma((pairs,)), dma((pairs,)), dma((pairs,)), dma((pairs,)),
+            *[dma((pairs, PIECES)) for _ in range(4)],
         ],
         compiler_params=pltpu.CompilerParams(
-            collective_id=1, has_side_effects=True, vmem_limit_bytes=VMEM_LIMIT
+            collective_id=1, has_side_effects=True, vmem_limit_bytes=REDUCE_VMEM * MIB
+        ),
+        cost_estimate=pl.CostEstimate(
+            flops=2 * count * units * model, bytes_accessed=100 * MIB, transcendentals=0
         ),
     )(hidden, down_columns)
     return (up_block, down_columns, mixed)

time: 118 us -> 107 us (0.907)
  Pallas kernels: 108 us -> 95.5 us
  local copies, waits for them, and re-layouts: 9.01 us -> 10.2 us
    pallas_call x1, Pallas kernels: 45.5 us -> 39 us  [per_device(): pl.pallas_call(reduce_kernel, out_shape=jax.ShapeDtypeStruct((count, wide...]
    pallas_call x1, Pallas kernels: 62.8 us -> 56.5 us  [per_device(): pl.pallas_call(functools.partial(gather_kernel, tp, blocks, fs), out_shap...]
    unnamed x7 -> x11, local copies, waits for them, and re-layouts: 7.54 us -> 10.2 us
    broadcast_in_dim x1 -> x0, local copies, waits for them, and re-layouts: 1.47 us -> none  [per_device(): norm_gain[:, None]]
where the time goes in v2:
time: 107 us; the launch traced here: 106 us
  Pallas kernels  95.5 us (89%)
  local copies, waits for them, and re-layouts  10.2 us (10%)
    pallas_call x1, Pallas kernels, per_device(): pl.pallas_call(functools.partial(gather_kernel, tp, blocks, fs), out_shap...  56.5 us
    pallas_call x1, Pallas kernels, per_device(): pl.pallas_call(reduce_kernel, out_shape=jax.ShapeDtypeStruct((count, wide...  39 us
    unnamed x11, local copies, waits for them, and re-layouts  10.2 us

profile of v2, /device:TPU:0, one launch (start us, length us, event | category | flops | bytes accessed | tf_op | source)
XLA Modules:
  0.0 106.3 jit_solution(9366822439166939784)
XLA Ops:
  0.6 0.0 copy-start
  0.6 1.6 %copy-done = bf16[512,2048]{1,0:T(8,128)(2,1)S(1)} copy-done((bf16[512,2048]{1,0:T(8,128)(2,1)S(1)}, bf16[512,2048]{1,0:T(8,128)(2,1)}, u32[]{:S(2)}) %copy-start) | copy-done | bytes 2097176
  2.2 0.0 copy-start.1
  2.2 1.6 %copy-done.1 = f32[256,2048]{1,0:T(8,128)S(1)} copy-done((f32[256,2048]{1,0:T(8,128)S(1)}, f32[256,2048]{1,0:T(8,128)}, u32[]{:S(2)}) %copy-start.1) | copy-done | bytes 2097176
  3.8 0.0 copy-start.2
  3.8 1.6 %copy-done.2 = f32[1024,512]{1,0:T(8,128)S(1)} copy-done((f32[1024,512]{1,0:T(8,128)S(1)}, f32[1024,512]{1,0:T(8,128)}, u32[]{:S(2)}) %copy-start.2) | copy-done | bytes 2097176
  5.4 0.0 copy-start.3
  5.4 0.7 copy-done.3
  6.1 56.5 %shard_map.67 = (bf16[2048,1024]{1,0:T(8,128)(2,1)S(1)}, bf16[1024,2048]{1,0:T(8,128)(2,1)S(1)}, bf16[512,1024]{1,0:T(8,128)(2,1)S(1)}) custom-call(bf16[512,2048]{1,0:T(8,128)(2,1)S(1)} %copy-done, f32[1,256]{1,0:T(1,128)S(1)} %bitcast.1, f32[256,2048]{1,0:T(8,128)S(1)} %copy-done.1, f32[1024,512]{1,0:T(8,128)S(1)} %copy-done.2), custom_call_target="tpu_custom_call" | custom-call | flops 2147483648 | bytes 167772160 | tf_op jit(solution)/shard_map/pallas_call | solution.py:297
  62.6 39.0 %shard_map.68 = bf16[512,256]{1,0:T(8,128)(2,1)S(1)} custom-call(bf16[512,1024]{1,0:T(8,128)(2,1)S(1)} %get-tuple-element.8.hidden, bf16[1024,2048]{1,0:T(8,128)(2,1)S(1)} %get-tuple-element.13.down), custom_call_target="tpu_custom_call" | custom-call | flops 2147483648 | bytes 104857600 | tf_op jit(solution)/shard_map/pallas_call | solution.py:323
  101.6 2.0 %copy.10 = bf16[2048,1024]{1,0:T(8,128)(2,1)} copy(bf16[2048,1024]{1,0:T(8,128)(2,1)S(1)} %get-tuple-element.12) | data formatting | bytes 8388608
  103.6 2.0 %copy.11 = bf16[1024,2048]{1,0:T(8,128)(2,1)} copy(bf16[1024,2048]{1,0:T(8,128)(2,1)S(1)} %get-tuple-element.13.down) | data formatting | bytes 8388608
  105.6 0.7 copy.12
Async XLA Ops:
  0.6 1.6 %copy-start = (bf16[512,2048]{1,0:T(8,128)(2,1)S(1)}, bf16[512,2048]{1,0:T(8,128)(2,1)}, u32[]{:S(2)}) copy-start(bf16[512,2048]{1,0:T(8,128)(2,1)} %tokens.1) | copy-start | bytes 6291460
  2.2 1.6 %copy-start.1 = (f32[256,2048]{1,0:T(8,128)S(1)}, f32[256,2048]{1,0:T(8,128)}, u32[]{:S(2)}) copy-start(f32[256,2048]{1,0:T(8,128)} %up.1) | copy-start | bytes 6291460
  3.8 1.6 %copy-start.2 = (f32[1024,512]{1,0:T(8,128)S(1)}, f32[1024,512]{1,0:T(8,128)}, u32[]{:S(2)}) copy-start(f32[1024,512]{1,0:T(8,128)} %down.1) | copy-start | bytes 6291460
  5.4 0.7 copy-start.3

commit v3 on v2

--- a/solution.py
+++ b/solution.py
@@ -10,8 +10,9 @@
 MESH = pl.DeviceIdType.MESH
 MIB = 1024 * 1024
 GATHER_VMEM = 32
+PARTIAL_VMEM = 20
 REDUCE_VMEM = 20
-SLICES = 2
+SLICE_ROWS = 32
 PIECES = 2
 
 
@@ -34,9 +35,17 @@
 
 
 def gather_kernel(
-    tp, blocks, shards, tokens, gain, up, down, up_out, down_out, hidden_out,
-    gath, normed, acc, xs, xr, fsend, frecv, ps, pr, ds_, dr, pds, pdr,
+    tp, blocks, shards, tokens_in, gain_in, up_in, down_in, up_out, down_out, hidden_out,
+    tokens, gain, up, down, loads, gath, normed, acc, xs, xr, fsend, frecv, ps, pr, ds_, dr, pds, pdr,
 ):
+    load = [
+        pltpu.make_async_copy(source, kept, loads.at[i])
+        for i, (source, kept) in enumerate(
+            [(gain_in, gain), (up_in, up), (down_in, down), (tokens_in, tokens)]
+        )
+    ]
+    for copy in load:
+        copy.start()
     g, f, t = lax.axis_index("gr"), lax.axis_index("fs"), lax.axis_index("tp")
     per = tp // 2
     chips = gath.shape[0]
@@ -67,10 +76,13 @@
                 barrier, inc=1, device_id=dev(c, other, core_id), device_id_type=MESH
             )
 
+    load[0].wait()
     square = (rows, rows)
     diagonal = lax.broadcasted_iota(jnp.int32, square, 0) == lax.broadcasted_iota(jnp.int32, square, 1)
     column = jnp.sum(jnp.where(diagonal, gain[...], 0.0), axis=1, keepdims=True)
+    load[1].wait()
     gath[c] = (column * up[...]).astype(jnp.bfloat16)
+    load[2].wait()
     down_out[:, down_cols(c, k)] = down[...].astype(jnp.bfloat16)
     pl.semaphore_wait(barrier, chips - 1 + 2 * shards - 1)
 
@@ -137,6 +149,7 @@
         down_copy(s).start()
     down_relay(0, k).start()
 
+    load[3].wait()
     widened = tokens[...].astype(jnp.float32)
     scale = lax.rsqrt(jnp.mean(widened * widened, axis=-1, keepdims=True) + 1e-06)
     for shard in range(shards):
@@ -210,7 +223,26 @@
                 forward(chip, j, h).wait_send()
 
 
-def reduce_kernel(hidden, down, mixed, part, ybuf, zout, zbuf, ys, yr, zs, zr):
+def partial_kernel(hidden, up, down, up_out, down_out, part, sems):
+    copies = [
+        pltpu.make_async_copy(up, up_out, sems.at[0]),
+        pltpu.make_async_copy(down, down_out, sems.at[1]),
+    ]
+    for copy in copies:
+        copy.start()
+    shards, _, wide = part.shape
+    for pair in range(shards // 2):
+        both = jnp.dot(
+            hidden[...], down[:, 2 * pair * wide:2 * (pair + 1) * wide],
+            preferred_element_type=jnp.float32,
+        ).astype(jnp.bfloat16)
+        part[2 * pair] = both[:, :wide]
+        part[2 * pair + 1] = both[:, wide:]
+    for copy in copies:
+        copy.wait()
+
+
+def reduce_kernel(part, mixed, ybuf, zout, zbuf, ys, yr, zs, zr):
     g, f, t = lax.axis_index("gr"), lax.axis_index("fs"), lax.axis_index("tp")
     pairs = ybuf.shape[0]
     wide = mixed.shape[1]
@@ -226,13 +258,6 @@
         )
     order = [flipped(z, s, pairs) for s in list(range(pairs - 1, 0, -1)) + [0]]
 
-    def compute(pair):
-        columns = pl.ds(pl.multiple_of(pair * 2 * wide, 2 * wide), 2 * wide)
-        both = jnp.dot(hidden[...], down[:, columns], preferred_element_type=jnp.float32)
-        both = both.astype(jnp.bfloat16)
-        part[2 * pair] = both[:, :wide]
-        part[2 * pair + 1] = both[:, wide:]
-
     pieces = ys.shape[1]
     span = mixed.shape[0] // pieces
 
@@ -250,13 +275,10 @@
             (g, pair * 2 + y, t),
         )
 
-    compute(order[0])
     pl.semaphore_wait(barrier, pairs)
-    for position in range(1, pairs + 1):
-        if position < pairs:
-            compute(order[position])
+    for pair in order:
         for i in range(pieces):
-            across(order[position - 1], i).start()
+            across(pair, i).start()
 
     def summed(pair, i):
         tokens = pl.ds(i * span, span)
@@ -287,11 +309,13 @@
     units, cols = down_weight.shape
     group = gr * tp
     chips = group // 2
+    slices = max(1, rows // 2 // SLICE_ROWS)
     block = width * group // fs
     blocks = width // block
     count, depth = tokens.shape
     model = cols * group
     vmem = pl.BlockSpec(memory_space=pltpu.VMEM)
+    hbm = pl.BlockSpec(memory_space=pltpu.HBM)
     bf16, f32 = jnp.bfloat16, jnp.float32
     dma = pltpu.SemaphoreType.DMA
     up_block, down_columns, hidden = pl.pallas_call(
@@ -301,13 +325,18 @@
             jax.ShapeDtypeStruct((units, model), bf16),
             jax.ShapeDtypeStruct((count, block), bf16),
         ),
-        in_specs=[vmem] * 4,
+        in_specs=[hbm] * 4,
         out_specs=(vmem,) * 3,
         scratch_shapes=[
+            pltpu.VMEM(tokens.shape, bf16),
+            pltpu.VMEM((1, rows), f32),
+            pltpu.VMEM(up_weight.shape, f32),
+            pltpu.VMEM(down_weight.shape, f32),
+            dma((4,)),
             pltpu.VMEM((chips, rows, width), bf16),
             pltpu.VMEM((fs, count, rows), bf16),
             pltpu.VMEM((count, block), f32),
-            *[dma((chips, blocks, 2 * SLICES)) for _ in range(3)], dma((fs,)),
+            *[dma((chips, blocks, 2 * slices)) for _ in range(3)], dma((fs,)),
             dma((fs,)), dma((fs,)),
             dma((chips,)), dma((chips,)), dma((chips,)), dma((chips,)),
         ],
@@ -317,16 +346,30 @@
         cost_estimate=pl.CostEstimate(
             flops=2 * count * depth * block, bytes_accessed=160 * MIB, transcendentals=0
         ),
-    )(tokens, norm_gain[None, :], up_weight, down_weight)
+    )(*[pltpu.with_memory_space_constraint(x, pltpu.HBM) for x in (tokens, norm_gain[None, :], up_weight, down_weight)])
     pairs = fs // 2
     wide = model // fs
+    up_block, down_columns, part = pl.pallas_call(
+        partial_kernel,
+        out_shape=(
+            jax.ShapeDtypeStruct(up_block.shape, bf16),
+            jax.ShapeDtypeStruct(down_columns.shape, bf16),
+            jax.ShapeDtypeStruct((fs, count, wide), bf16),
+        ),
+        in_specs=[vmem] * 3,
+        out_specs=(hbm, hbm, vmem),
+        scratch_shapes=[dma((2,))],
+        compiler_params=pltpu.CompilerParams(vmem_limit_bytes=PARTIAL_VMEM * MIB),
+        cost_estimate=pl.CostEstimate(
+            flops=2 * count * units * model, bytes_accessed=16 * MIB, transcendentals=0
+        ),
+    )(hidden, up_block, down_columns)
     mixed = pl.pallas_call(
         reduce_kernel,
         out_shape=jax.ShapeDtypeStruct((count, wide), bf16),
-        in_specs=[vmem] * 2,
+        in_specs=[vmem],
         out_specs=vmem,
         scratch_shapes=[
-            pltpu.VMEM((fs, count, wide), bf16),
             pltpu.VMEM((pairs, count, wide), bf16),
             pltpu.VMEM((pairs, count, wide), bf16),
             pltpu.VMEM((pairs, count, wide), bf16),
@@ -336,9 +379,9 @@
             collective_id=1, has_side_effects=True, vmem_limit_bytes=REDUCE_VMEM * MIB
         ),
         cost_estimate=pl.CostEstimate(
-            flops=2 * count * units * model, bytes_accessed=100 * MIB, transcendentals=0
-        ),
-    )(hidden, down_columns)
+            flops=count * model, bytes_accessed=100 * MIB, transcendentals=0
+        ),
+    )(part)
     return (up_block, down_columns, mixed)
 
 

time: 107 us -> 98.9 us (0.924)
  local copies, waits for them, and re-layouts: 10.2 us -> 0.71 us
  Pallas kernels: 95.5 us -> 97.4 us
    unnamed x11 -> x1, local copies, waits for them, and re-layouts: 10.2 us -> 0.71 us
    pallas_call x1, Pallas kernels: 39 us -> 35.2 us  [per_device(): pl.pallas_call(reduce_kernel, out_shape=jax.ShapeDtypeStruct((count, wide...]
    pallas_call x0 -> x1, Pallas kernels: none -> 3.41 us  [per_device(): pl.pallas_call(partial_kernel, out_shape=(jax.ShapeDtypeStruct(up_block.s...]
    pallas_call x1, Pallas kernels: 56.5 us -> 58.8 us  [per_device(): pl.pallas_call(functools.partial(gather_kernel, tp, blocks, fs), out_shap...]
where the time goes in v3:
time: 98.9 us; the launch traced here: 98.8 us
  Pallas kernels  97.4 us (98%)
    pallas_call x1, Pallas kernels, per_device(): pl.pallas_call(functools.partial(gather_kernel, tp, blocks, fs), out_shap...  58.8 us
    pallas_call x1, Pallas kernels, per_device(): pl.pallas_call(reduce_kernel, out_shape=jax.ShapeDtypeStruct((count, wide...  35.2 us
    pallas_call x1, Pallas kernels, per_device(): pl.pallas_call(partial_kernel, out_shape=(jax.ShapeDtypeStruct(up_block.s...  3.41 us

profile of v3, /device:TPU:0, one launch (start us, length us, event | category | flops | bytes accessed | tf_op | source)
XLA Modules:
  0.0 98.8 jit_solution(10885051095141170184)
XLA Ops:
  0.6 58.8 %shard_map.67 = (bf16[2048,1024]{1,0:T(8,128)(2,1)S(1)}, bf16[1024,2048]{1,0:T(8,128)(2,1)S(1)}, bf16[512,1024]{1,0:T(8,128)(2,1)S(1)}) custom-call(bf16[512,2048]{1,0:T(8,128)(2,1)} %tokens_in.1, f32[1,256]{1,0:T(1,128)} %bitcast.1, f32[256,2048]{1,0:T(8,128)} %up_in.1, f32[1024,512]{1,0:T(8,128)} %down_in.1), custom_call_target="tpu_custom_call" | custom-call | flops 2147483648 | bytes 167772160 | tf_op jit(solution)/shard_map/pallas_call | solution.py:321
  59.4 3.4 %shard_map.68 = (bf16[2048,1024]{1,0:T(8,128)(2,1)}, bf16[1024,2048]{1,0:T(8,128)(2,1)}, bf16[8,512,256]{2,1,0:T(8,128)(2,1)S(1)}) custom-call(bf16[512,1024]{1,0:T(8,128)(2,1)S(1)} %get-tuple-element.9.hidden, bf16[2048,1024]{1,0:T(8,128)(2,1)S(1)} %get-tuple-element.10.up, bf16[1024,2048]{1,0:T(8,128)(2,1)S(1)} %get-tuple-element.11.down), custom_call_target="tpu_custom_call" | custom-call | flops 2147483648 | bytes 16777216 | tf_op jit(solution)/shard_map/pallas_call | solution.py:352
  62.8 35.2 %shard_map.69 = bf16[512,256]{1,0:T(8,128)(2,1)S(1)} custom-call(bf16[8,512,256]{2,1,0:T(8,128)(2,1)S(1)} %get-tuple-element.14.part), custom_call_target="tpu_custom_call" | custom-call | flops 1048576 | bytes 104857600 | tf_op jit(solution)/shard_map/pallas_call | solution.py:367
  98.1 0.7 copy.8

commit v4 on v3

--- a/solution.py
+++ b/solution.py
@@ -13,7 +13,7 @@
 PARTIAL_VMEM = 20
 REDUCE_VMEM = 20
 SLICE_ROWS = 32
-PIECES = 2
+PIECES = 4
 
 
 def flipped(index, step, count):
@@ -242,11 +242,18 @@
         copy.wait()
 
 
-def reduce_kernel(part, mixed, ybuf, zout, zbuf, ys, yr, zs, zr):
+def reduce_kernel(part, mixed, ybuf, zout, zbuf, gbuf, ys, yr, zs, zr, gr_sem):
     g, f, t = lax.axis_index("gr"), lax.axis_index("fs"), lax.axis_index("tp")
-    pairs = ybuf.shape[0]
-    wide = mixed.shape[1]
+    pairs, pieces = ys.shape
+    side = pairs // 2
+    span = mixed.shape[0] // pieces
     z, y = f // 2, lax.rem(f, 2)
+    upper, odd = z // side, lax.rem(z, 2)
+    is_gate = lax.rem(odd + upper, 2) == 1
+    mate = z + 1 - 2 * odd
+    far = [(1 - upper) * side + i for i in range(side)]
+    near = [upper * side + lax.rem(lax.rem(z, side) + s, side) for s in range(1, side)]
+    far_gates = [(1 - upper) * side + 2 * i + upper for i in range(side // 2)]
 
     barrier = pltpu.get_barrier_semaphore()
     pl.semaphore_signal(
@@ -256,51 +263,68 @@
         pl.semaphore_signal(
             barrier, inc=1, device_id=(g, lax.rem(z + s, pairs) * 2 + y, t), device_id_type=MESH
         )
-    order = [flipped(z, s, pairs) for s in list(range(pairs - 1, 0, -1)) + [0]]
-
-    pieces = ys.shape[1]
-    span = mixed.shape[0] // pieces
+    rows = [pl.ds(i * span, span) for i in range(pieces)]
 
     def across(pair, i):
-        tokens = pl.ds(i * span, span)
-        return remote(
-            part.at[2 * pair + 1 - y, tokens], ybuf.at[pair, tokens], ys.at[pair, i],
+        return remote(
+            part.at[2 * pair + 1 - y, rows[i]], ybuf.at[pair, rows[i]], ys.at[pair, i],
             yr.at[pair, i], (g, z * 2 + 1 - y, t),
         )
 
     def along(pair, sender, i):
-        tokens = pl.ds(i * span, span)
-        return remote(
-            zout.at[pair, tokens], zbuf.at[sender, tokens], zs.at[pair, i], zr.at[sender, i],
+        return remote(
+            zout.at[pair, rows[i]], zbuf.at[sender, rows[i]], zs.at[pair, i], zr.at[sender, i],
             (g, pair * 2 + y, t),
         )
 
+    def to_mate(pair, i):
+        return remote(
+            zout.at[pair, rows[i]], gbuf.at[pair, rows[i]], zs.at[pair, i], gr_sem.at[pair, i],
+            (g, mate * 2 + y, t),
+        )
+
     pl.semaphore_wait(barrier, pairs)
-    for pair in order:
+    for pair in far + near + [z]:
         for i in range(pieces):
             across(pair, i).start()
 
     def summed(pair, i):
-        tokens = pl.ds(i * span, span)
-        return part[2 * pair + y, tokens].astype(jnp.float32) + ybuf[pair, tokens].astype(jnp.float32)
-
-    for pair in order[:-1]:
+        return part[2 * pair + y, rows[i]].astype(jnp.float32) + ybuf[pair, rows[i]].astype(jnp.float32)
+
+    @pl.when(is_gate)
+    def _():
+        for pair in far:
+            for i in range(pieces):
+                across(pair, i).wait_recv()
+                to_mate(pair, i).wait_recv()
+                total = summed(pair, i) + gbuf[pair, rows[i]].astype(jnp.float32)
+                zout[pair, rows[i]] = total.astype(jnp.bfloat16)
+                along(pair, z, i).start()
+
+    @pl.when(jnp.logical_not(is_gate))
+    def _():
+        for pair in far:
+            for i in range(pieces):
+                across(pair, i).wait_recv()
+                zout[pair, rows[i]] = summed(pair, i).astype(jnp.bfloat16)
+                to_mate(pair, i).start()
+
+    for pair in near:
         for i in range(pieces):
             across(pair, i).wait_recv()
-            zout[pair, pl.ds(i * span, span)] = summed(pair, i).astype(jnp.bfloat16)
+            zout[pair, rows[i]] = summed(pair, i).astype(jnp.bfloat16)
             along(pair, z, i).start()
     for i in range(pieces):
-        tokens = pl.ds(i * span, span)
         across(z, i).wait_recv()
         total = summed(z, i)
-        for pair in order[:-1]:
-            along(z, pair, i).wait_recv()
-            total = total + zbuf[pair, tokens].astype(jnp.float32)
-        mixed[tokens] = total.astype(jnp.bfloat16)
+        for sender in far_gates + near:
+            along(z, sender, i).wait_recv()
+            total = total + zbuf[sender, rows[i]].astype(jnp.float32)
+        mixed[rows[i]] = total.astype(jnp.bfloat16)
     for i in range(pieces):
-        for pair in order:
+        for pair in far + near + [z]:
             across(pair, i).wait_send()
-        for pair in order[:-1]:
+        for pair in far + near:
             along(pair, z, i).wait_send()
 
 
@@ -373,7 +397,8 @@
             pltpu.VMEM((pairs, count, wide), bf16),
             pltpu.VMEM((pairs, count, wide), bf16),
             pltpu.VMEM((pairs, count, wide), bf16),
-            *[dma((pairs, PIECES)) for _ in range(4)],
+            pltpu.VMEM((pairs, count, wide), bf16),
+            *[dma((pairs, PIECES)) for _ in range(5)],
         ],
         compiler_params=pltpu.CompilerParams(
             collective_id=1, has_side_effects=True, vmem_limit_bytes=REDUCE_VMEM * MIB

time: 98.9 us -> 95 us (0.961)
  Pallas kernels: 97.4 us -> 93.5 us
    pallas_call x1, Pallas kernels: 35.2 us -> 31.3 us  [per_device(): pl.pallas_call(reduce_kernel, out_shape=jax.ShapeDtypeStruct((count, wide...]
where the time goes in v4:
time: 95 us; the launch traced here: 94.9 us
  Pallas kernels  93.5 us (98%)
    pallas_call x1, Pallas kernels, per_device(): pl.pallas_call(functools.partial(gather_kernel, tp, blocks, fs), out_shap...  58.8 us
    pallas_call x1, Pallas kernels, per_device(): pl.pallas_call(reduce_kernel, out_shape=jax.ShapeDtypeStruct((count, wide...  31.3 us
    pallas_call x1, Pallas kernels, per_device(): pl.pallas_call(partial_kernel, out_shape=(jax.ShapeDtypeStruct(up_block.s...  3.41 us

profile of v4, /device:TPU:0, one launch (start us, length us, event | category | flops | bytes accessed | tf_op | source)
XLA Modules:
  0.0 94.9 jit_solution(2210212036119685097)
XLA Ops:
  0.6 58.8 %shard_map.67 = (bf16[2048,1024]{1,0:T(8,128)(2,1)S(1)}, bf16[1024,2048]{1,0:T(8,128)(2,1)S(1)}, bf16[512,1024]{1,0:T(8,128)(2,1)S(1)}) custom-call(bf16[512,2048]{1,0:T(8,128)(2,1)} %tokens_in.1, f32[1,256]{1,0:T(1,128)} %bitcast.1, f32[256,2048]{1,0:T(8,128)} %up_in.1, f32[1024,512]{1,0:T(8,128)} %down_in.1), custom_call_target="tpu_custom_call" | custom-call | flops 2147483648 | bytes 167772160 | tf_op jit(solution)/shard_map/pallas_call | solution.py:345
  59.4 3.4 %shard_map.68 = (bf16[2048,1024]{1,0:T(8,128)(2,1)}, bf16[1024,2048]{1,0:T(8,128)(2,1)}, bf16[8,512,256]{2,1,0:T(8,128)(2,1)S(1)}) custom-call(bf16[512,1024]{1,0:T(8,128)(2,1)S(1)} %get-tuple-element.9.hidden, bf16[2048,1024]{1,0:T(8,128)(2,1)S(1)} %get-tuple-element.10.up, bf16[1024,2048]{1,0:T(8,128)(2,1)S(1)} %get-tuple-element.11.down), custom_call_target="tpu_custom_call" | custom-call | flops 2147483648 | bytes 16777216 | tf_op jit(solution)/shard_map/pallas_call | solution.py:376
  62.8 31.3 %shard_map.69 = bf16[512,256]{1,0:T(8,128)(2,1)S(1)} custom-call(bf16[8,512,256]{2,1,0:T(8,128)(2,1)S(1)} %get-tuple-element.14.part), custom_call_target="tpu_custom_call" | custom-call | flops 1048576 | bytes 104857600 | tf_op jit(solution)/shard_map/pallas_call | solution.py:391
  94.2 0.7 copy.8

commit v5 on v4

--- a/solution.py
+++ b/solution.py
@@ -82,8 +82,6 @@
     column = jnp.sum(jnp.where(diagonal, gain[...], 0.0), axis=1, keepdims=True)
     load[1].wait()
     gath[c] = (column * up[...]).astype(jnp.bfloat16)
-    load[2].wait()
-    down_out[:, down_cols(c, k)] = down[...].astype(jnp.bfloat16)
     pl.semaphore_wait(barrier, chips - 1 + 2 * shards - 1)
 
     slices = xs.shape[2] // 2
@@ -145,9 +143,17 @@
         for s in range(1, chips):
             exchange(s, j, h).start()
         start_forward(c, j, h)
-    for s in range(1, chips):
-        down_copy(s).start()
-    down_relay(0, k).start()
+    for index, (j, h) in enumerate(units):
+        if index == len(units) // 2:
+            load[2].wait()
+            down_out[:, down_cols(c, k)] = down[...].astype(jnp.bfloat16)
+        if index == 3 * len(units) // 4:
+            for s in range(1, chips):
+                down_copy(s).start()
+            down_relay(0, k).start()
+        for s in range(1, chips):
+            exchanged(s, j, h).wait_recv()
+            start_forward(lax.rem(c + chips - s, chips), j, h)
 
     load[3].wait()
     widened = tokens[...].astype(jnp.float32)
@@ -155,11 +161,6 @@
     for shard in range(shards):
         part = tokens[:, shard * rows:(shard + 1) * rows].astype(jnp.float32)
         normed[shard] = (part * scale).astype(jnp.bfloat16)
-
-    for j, h in units:
-        for s in range(1, chips):
-            exchanged(s, j, h).wait_recv()
-            start_forward(lax.rem(c + chips - s, chips), j, h)
 
     source_core = lax.rem(f // blocks, 2)
     own_stays = source_core == k

time: 95 us -> 95 us (level)
  no operation moved by 1% of the time
where the time goes in v5:
time: 95 us; the launch traced here: 94.9 us
  Pallas kernels  93.5 us (98%)
    pallas_call x1, Pallas kernels, per_device(): pl.pallas_call(functools.partial(gather_kernel, tp, blocks, fs), out_shap...  58.3 us
    pallas_call x1, Pallas kernels, per_device(): pl.pallas_call(reduce_kernel, out_shape=jax.ShapeDtypeStruct((count, wide...  31.8 us
    pallas_call x1, Pallas kernels, per_device(): pl.pallas_call(partial_kernel, out_shape=(jax.ShapeDtypeStruct(up_block.s...  3.41 us

profile of v5, /device:TPU:0, one launch (start us, length us, event | category | flops | bytes accessed | tf_op | source)
XLA Modules:
  0.0 94.9 jit_solution(6760105121532619168)
XLA Ops:
  0.6 58.3 %shard_map.67 = (bf16[2048,1024]{1,0:T(8,128)(2,1)S(1)}, bf16[1024,2048]{1,0:T(8,128)(2,1)S(1)}, bf16[512,1024]{1,0:T(8,128)(2,1)S(1)}) custom-call(bf16[512,2048]{1,0:T(8,128)(2,1)} %tokens_in.1, f32[1,256]{1,0:T(1,128)} %bitcast.1, f32[256,2048]{1,0:T(8,128)} %up_in.1, f32[1024,512]{1,0:T(8,128)} %down_in.1), custom_call_target="tpu_custom_call" | custom-call | flops 2147483648 | bytes 167772160 | tf_op jit(solution)/shard_map/pallas_call | solution.py:346
  58.9 3.4 %shard_map.68 = (bf16[2048,1024]{1,0:T(8,128)(2,1)}, bf16[1024,2048]{1,0:T(8,128)(2,1)}, bf16[8,512,256]{2,1,0:T(8,128)(2,1)S(1)}) custom-call(bf16[512,1024]{1,0:T(8,128)(2,1)S(1)} %get-tuple-element.9.hidden, bf16[2048,1024]{1,0:T(8,128)(2,1)S(1)} %get-tuple-element.10.up, bf16[1024,2048]{1,0:T(8,128)(2,1)S(1)} %get-tuple-element.11.down), custom_call_target="tpu_custom_call" | custom-call | flops 2147483648 | bytes 16777216 | tf_op jit(solution)/shard_map/pallas_call | solution.py:377
  62.4 31.8 %shard_map.69 = bf16[512,256]{1,0:T(8,128)(2,1)S(1)} custom-call(bf16[8,512,256]{2,1,0:T(8,128)(2,1)S(1)} %get-tuple-element.14.part), custom_call_target="tpu_custom_call" | custom-call | flops 1048576 | bytes 104857600 | tf_op jit(solution)/shard_map/pallas_call | solution.py:392
  94.2 0.7 copy.8
